TPU v7x, 32 devices: a whole 2x2x4 slice. The times are simulated.
32 devices in a mesh: grp: 2 (over y), ep: 4 (over z), tp: 4 (over x, core).
Axes of the slice: x: 2, y: 2, z: 4, core: 2. Of those that a mesh axis runs over, the one named last changes fastest.
Arguments:
- x_in: bfloat16 [512, 2048], P(('grp', 'ep')), parts along dimension 0, may hold values from -6 to 6
- state: float32 [512, 96, 128], P(('grp', 'ep'), 'tp'), parts along dimension 0, may hold values from -6 to 6
- routes: int32 [512, 2], P(('grp', 'ep')), parts along dimension 0, may hold values from 0 to 7, as said below
- w_in: bfloat16 [2048, 1536], P(None, 'tp'), may hold values from -0.125 to 0.125
- decay_rate: float32 [96, 64], P('tp'), may hold values from 0.01 to 1
- frequency: float32 [96, 64], P('tp'), may hold values from 0 to 192
- log_step: float32 [96], P('tp'), may hold values from -3 to 0
- b_in: float32 [96, 16, 128], P('tp'), may hold values from -1.5 to 1.5
- c_out: float32 [96, 16, 128], P('tp'), may hold values from -0.5 to 0.5
- skip: float32 [1536], P('tp'), may hold values from -3 to 3
- w_out: bfloat16 [1536, 2048], P('tp'), may hold values from -0.15625 to 0.15625
- gain_mix: float32 [2048], replicated, may hold values from 0.1 to 1.9
- w_group: bfloat16 [2048, 4], replicated, may hold values from -0.0625 to 0.0625
- w_expert: bfloat16 [2048, 8], replicated, may hold values from -0.0625 to 0.0625
- w_gate: bfloat16 [8, 2048, 1024], P('ep', None, 'tp'), may hold values from -0.125 to 0.125
- w_up: bfloat16 [8, 2048, 1024], P('ep', None, 'tp'), may hold values from -0.125 to 0.125
- w_down: bfloat16 [8, 1024, 2048], P('ep', 'tp'), may hold values from -3 to 3
- gain_moe: float32 [2048], replicated, may hold values from 0.1 to 1.9
Outputs:
- layer_out: bfloat16 [512, 2048], P(('grp', 'ep')), parts along dimension 0
- new_state: float32 [512, 96, 128], P(('grp', 'ep'), 'tp'), parts along dimension 0
There are 2 independent parts, one for each index of `grp`. A program takes and returns all parts, laid end to end along the dimension named above; an argument that names none is the same for every part. Nothing has to cross between parts.
Inputs may be any that keep to these rules, and one draw needn't show every extreme that they name: `routes`: each row names two different experts of one group of 2 consecutive expert numbers. Within the rows of one index of ep (aligned blocks of 64 rows) no expert is named by more than 32 rows, and in every block some expert is named by exactly 32 rows.
All inputs are finite; a program needn't handle non-finite values.
Results may differ from a plain program's by a relative error of at most 0.015.
Values may be sent and summed in bfloat16 or wider, within the bound.
A program may use at most 64 MiB of HBM per device.

v0:
```python
import functools
import math

import jax
import jax.numpy as jnp
from jax import lax
from jax.experimental import pallas as pl
from jax.experimental.pallas import tpu as pltpu
from jax.sharding import PartitionSpec as P

residual_scale = 8.0**0.25
norm_eps = 1e-05


def normalize(values, gain):
    centre = jnp.mean(values, -1, keepdims=True)
    spread = jnp.mean(jnp.square(values - centre), -1, keepdims=True)
    return (values - centre) * lax.rsqrt(spread + norm_eps) * gain


def s5_advance(mix_input, state, decay_rate, frequency, log_step, b_in, c_out, skip):
    top_precision = lax.Precision.HIGHEST
    entries = decay_rate.shape[-1]
    group_count = decay_rate.shape[0]
    width = b_in.shape[1]
    seq_count = mix_input.shape[0]
    input_rows = mix_input.astype(jnp.float32).reshape(seq_count, group_count, width)
    step_size = jnp.exp(log_step)[:, None]
    lam_real = -decay_rate
    magnitude = jnp.exp(lam_real * step_size)
    angle_dt = frequency * step_size
    bar_real = magnitude * jnp.cos(angle_dt)
    bar_imag = magnitude * jnp.sin(angle_dt)
    minus_real = bar_real - 1.0
    modulus = lam_real * lam_real + frequency * frequency
    ratio_real = (minus_real * lam_real + bar_imag * frequency) / modulus
    ratio_imag = (bar_imag * lam_real - minus_real * frequency) / modulus
    in_real = b_in[..., :entries]
    in_imag = b_in[..., entries:]
    input_matrix_real = ratio_real[:, None, :] * in_real - ratio_imag[:, None, :] * in_imag
    input_matrix_imag = ratio_real[:, None, :] * in_imag + ratio_imag[:, None, :] * in_real
    forcing_real = jnp.einsum(
        "rxf,xfb->rxb", input_rows, input_matrix_real, precision=top_precision
    )
    forcing_imag = jnp.einsum(
        "rxf,xfb->rxb", input_rows, input_matrix_imag, precision=top_precision
    )
    old_real = state[..., :entries]
    old_imag = state[..., entries:]
    following_real = bar_real * old_real - bar_imag * old_imag + forcing_real
    following_imag = bar_real * old_imag + bar_imag * old_real + forcing_imag
    output_real = c_out[..., :entries]
    output_imag = c_out[..., entries:]
    output_matrix = jnp.einsum("lzt,zft->lzf", following_real, output_real, precision=top_precision)
    output_matrix = output_matrix - jnp.einsum(
        "lzt,zft->lzf", following_imag, output_imag, precision=top_precision
    )
    output_matrix = output_matrix + skip.reshape(group_count, width) * input_rows
    activated = jax.nn.gelu(output_matrix).reshape(seq_count, group_count * width)
    return (activated, jnp.concatenate([following_real, following_imag], axis=-1))


def route_weights(normed, routes, w_group, w_expert):
    group_total = w_group.shape[1]
    expert_total = w_expert.shape[1]
    per_group = expert_total // group_total
    group_logit = jnp.dot(normed, w_group, preferred_element_type=jnp.float32)
    group_exp = jnp.exp(group_logit)
    group_prob = group_exp / jnp.sum(group_exp, -1, keepdims=True)
    chosen = routes[:, 0] // per_group
    group_pick = jnp.sum(
        jnp.where(
            chosen[:, None] == jnp.arange(group_total, dtype=jnp.int32)[None, :], group_prob, 0.0
        ),
        -1,
    )
    expert_logit = jnp.dot(normed, w_expert, preferred_element_type=jnp.float32)
    picked = jnp.sum(
        jnp.where(
            routes[:, :, None] == jnp.arange(expert_total, dtype=jnp.int32)[None, None, :],
            expert_logit[:, None, :],
            0.0,
        ),
        -1,
    )
    pair_exp = jnp.exp(picked)
    return pair_exp / jnp.sum(pair_exp, -1, keepdims=True) * group_pick[:, None]


def per_device(
    x_in,
    state,
    routes,
    w_in,
    decay_rate,
    frequency,
    log_step,
    b_in,
    c_out,
    skip,
    w_out,
    gain_mix,
    w_group,
    w_expert,
    w_gate,
    w_up,
    w_down,
    gain_moe,
):
    top_precision = lax.Precision.HIGHEST
    seq_count = x_in.shape[0]
    model_width = x_in.shape[1]
    mix_input = jnp.dot(x_in, w_in, preferred_element_type=jnp.float32).astype(jnp.bfloat16)
    activated, new_state = s5_advance(
        mix_input, state, decay_rate, frequency, log_step, b_in, c_out, skip
    )
    partial_mix = jnp.dot(activated.astype(jnp.bfloat16), w_out, preferred_element_type=jnp.float32)
    mixed = lax.psum(partial_mix.astype(jnp.bfloat16), "tp").astype(jnp.float32)
    hidden_state = normalize(residual_scale * x_in.astype(jnp.float32) + mixed, gain_mix)
    hidden_bf = hidden_state.astype(jnp.bfloat16)
    route_weight = route_weights(hidden_bf, routes, w_group, w_expert)
    expert_total = w_expert.shape[1]
    ep_count = lax.axis_size("ep")
    local_experts = w_gate.shape[0]
    capacity = max(2, 4 * seq_count // expert_total)
    total_slots = expert_total * capacity
    hits = (routes[:, :, None] == jnp.arange(expert_total, dtype=jnp.int32)[None, None, :]).astype(
        jnp.int32
    )
    tally = jnp.sum(hits, axis=1)
    prior = jnp.cumsum(tally, axis=0) - tally
    slot_in_block = jnp.sum(prior[:, None, :] * hits, axis=-1)
    target = routes * capacity + slot_in_block
    slot_ids = jnp.arange(total_slots, dtype=jnp.int32)
    matches = target[:, :, None] == slot_ids[None, None, :]
    dispatch_map = jnp.any(slot_ids[:, None, None] == target[None, :, :], axis=-1).astype(
        jnp.bfloat16
    )
    combine_map = jnp.sum(jnp.where(matches, route_weight[:, :, None], 0.0), axis=1)
    buffer = jnp.dot(dispatch_map, hidden_bf, preferred_element_type=jnp.float32).astype(
        jnp.bfloat16
    )
    buffer = buffer.reshape(ep_count, local_experts, capacity, model_width)
    slot_rows = lax.all_to_all(buffer, "ep", split_axis=0, concat_axis=0, tiled=True)
    gate_val = jnp.einsum("njcd,jdf->njcf", slot_rows, w_gate, preferred_element_type=jnp.float32)
    up_val = jnp.einsum("njcd,jdf->njcf", slot_rows, w_up, preferred_element_type=jnp.float32)
    act = (jax.nn.silu(gate_val) * up_val).astype(jnp.bfloat16)
    share = lax.psum_scatter(
        jnp.einsum("njcf,jfd->njcd", act, w_down, preferred_element_type=jnp.float32).astype(
            jnp.bfloat16
        ),
        "tp",
        scatter_dimension=3,
        tiled=True,
    )
    returned_rows = lax.all_to_all(share, "ep", split_axis=0, concat_axis=0, tiled=True)
    flat_rows = returned_rows.reshape(total_slots, returned_rows.shape[3])
    moe = jnp.dot(
        combine_map,
        lax.all_gather(flat_rows, "tp", axis=1, tiled=True).astype(jnp.float32),
        precision=top_precision,
    )
    layer_out = normalize(residual_scale * hidden_state + moe, gain_moe).astype(jnp.bfloat16)
    return (layer_out, new_state)


MESH = pl.DeviceIdType.MESH


def sin_cos(angle):
    turns = jnp.floor(angle * (2.0 / math.pi) + 0.5)
    rest = ((angle - turns * 1.5703125) - turns * 4.837512969970703e-4) - turns * 7.549789954891882e-8
    square = rest * rest
    sine = rest + rest * square * (
        -1.6666654611e-1 + square * (8.3321608736e-3 - square * 1.9515295891e-4)
    )
    cosine = (
        1.0
        - 0.5 * square
        + square
        * square
        * (4.166664568298827e-2 + square * (-1.388731625493765e-3 + square * 2.443315711809948e-5))
    )
    quadrant = turns - 4.0 * jnp.floor(turns * 0.25)
    odd = (quadrant == 1.0) | (quadrant == 3.0)
    swapped_sine = jnp.where(odd, cosine, sine)
    swapped_cosine = jnp.where(odd, sine, cosine)
    out_sine = jnp.where(quadrant >= 2.0, -swapped_sine, swapped_sine)
    flip = (quadrant == 1.0) | (quadrant == 2.0)
    out_cosine = jnp.where(flip, -swapped_cosine, swapped_cosine)
    return out_sine, out_cosine


def nt_dot(left, right):
    return lax.dot_general(
        left, right, (((1,), (1,)), ((), ())), preferred_element_type=jnp.float32
    )


def f32_dot(left, right):
    return jnp.dot(left, right, preferred_element_type=jnp.float32)


def to_lanes(columns, rows):
    lane = lax.broadcasted_iota(jnp.int32, (rows, 128), 1)
    packed = jnp.zeros((rows, 128), jnp.float32)
    for at, column in enumerate(columns):
        packed = jnp.where(lane == at, column, packed)
    if rows < 128:
        packed = jnp.concatenate([packed, jnp.zeros((128 - rows, 128), jnp.float32)], 0)
    return packed.T[0:8]


def to_columns(lines, rows):
    row = lax.broadcasted_iota(jnp.int32, (128, 128), 0)
    packed = jnp.zeros((128, 128), jnp.float32)
    for at, line in enumerate(lines):
        packed = jnp.where(row == at, line, packed)
    return packed.T[:rows]


def fused_kernel(
    log_step,
    x_hbm, state_hbm, routes, w_in_hbm, decay, freq, b_hbm, c_hbm, skip, w_out_hbm,
    gain_mix, w_group, w_expert, w_gate_hbm, w_up_hbm, w_down_hbm, gain_moe,
    out_ref, new_state_hbm,
    x_ref, state, new_state, w_in, w_out, b_ref, c_ref, w_gate, w_up, w_down,
    b_blocks, c_blocks,
    mix_send, mix_recv, stat_mix, hidden_f32, go_rows, rows_all, line_all, line_columns,
    core_send, core_recv, cross_send, cross_recv, back_send, back_out, back_recv,
    out_parts, stat_out,
    local_sem,
    mix_ss, mix_rs, stat_ss, stat_rs, go_ss, go_rs, line_ss, line_rs, gather_ss, gather_rs,
    core_ss, core_rs, cross_ss, cross_rs, back_ss, back_rs,
    last_ss, last_rs, stat2_ss, stat2_rs,
):
    tp = lax.axis_index("tp")
    ep = lax.axis_index("ep")
    n_ep = lax.axis_size("ep")
    n_tp = 4
    seqs, width = x_ref.shape
    quarter = width // n_tp
    groups = decay.shape[0]
    entries = decay.shape[1]
    chans = b_ref.shape[0] // groups
    mix_dev = w_in.shape[1]
    cap = go_rows.shape[1]
    slots = n_ep * cap
    ff = w_gate.shape[2]
    experts = w_gate.shape[0]

    core = tp % 2
    chip = tp // 2
    peer = {
        0: tp,
        1: chip * 2 + (1 - core),
        2: (1 - chip) * 2 + core,
        3: (1 - chip) * 2 + (1 - core),
    }

    def tp_copy(src, dst, send_sem, recv_sem, k):
        return pltpu.make_async_remote_copy(
            src_ref=src, dst_ref=dst, send_sem=send_sem, recv_sem=recv_sem,
            device_id={"tp": peer[k]}, device_id_type=MESH,
        )

    def ep_copy(src, dst, send_sem, recv_sem, j):
        return pltpu.make_async_remote_copy(
            src_ref=src, dst_ref=dst, send_sem=send_sem, recv_sem=recv_sem,
            device_id={"ep": (ep + j) % n_ep}, device_id_type=MESH,
        )

    def columns(q):
        return pl.ds(pl.multiple_of(q * quarter, quarter), quarter)

    loads = {}
    for at, (name, src, dst) in enumerate((
        ("b", b_hbm, b_ref), ("c", c_hbm, c_ref), ("x", x_hbm, x_ref), ("w_in", w_in_hbm, w_in),
        ("state", state_hbm, state), ("w_out", w_out_hbm, w_out),
        ("gate", w_gate_hbm, w_gate), ("up", w_up_hbm, w_up), ("down", w_down_hbm, w_down),
    )):
        loads[name] = pltpu.make_async_copy(src, dst, local_sem.at[at])
        loads[name].start()

    barrier = pltpu.get_barrier_semaphore()
    for k in (1, 2, 3):
        pl.semaphore_signal(barrier, inc=1, device_id={"tp": peer[k]}, device_id_type=MESH)
    for j in range(1, n_ep):
        pl.semaphore_signal(
            barrier, inc=1, device_id={"ep": (ep + j) % n_ep}, device_id_type=MESH
        )

    group_row = lax.broadcasted_iota(jnp.int32, (groups, entries), 0)
    step_log = jnp.zeros((groups, entries), jnp.float32)
    for g in range(groups):
        step_log = jnp.where(group_row == g, log_step[g], step_log)
    step_size = jnp.exp(step_log)
    lam_real = -decay[...]
    lam_imag = freq[...]
    magnitude = jnp.exp(lam_real * step_size)
    sine, cosine = sin_cos(lam_imag * step_size)
    bar_real = magnitude * cosine
    bar_imag = magnitude * sine
    minus_real = bar_real - 1.0
    modulus = lam_real * lam_real + lam_imag * lam_imag
    ratio_real = (minus_real * lam_real + bar_imag * lam_imag) / modulus
    ratio_imag = (bar_imag * lam_real - minus_real * lam_imag) / modulus
    bar_same = jnp.concatenate([bar_real, bar_real], 1)
    bar_cross = jnp.concatenate([-bar_imag, bar_imag], 1)
    ratio_same = jnp.concatenate([ratio_real, ratio_real], 1)
    ratio_cross = jnp.concatenate([-ratio_imag, ratio_imag], 1)
    lanes = 2 * entries
    per_block = b_blocks.shape[2] // lanes
    blocks = b_blocks.shape[0]
    b_blocks[...] = jnp.zeros_like(b_blocks)
    c_blocks[...] = jnp.zeros_like(c_blocks)
    loads["b"].wait()
    loads["c"].wait()
    sign = jnp.where(lax.broadcasted_iota(jnp.int32, (chans, lanes), 1) < entries, 1.0, -1.0)
    for g in range(groups):
        block, j = g // per_block, g % per_block
        b_in = b_ref[g * chans:(g + 1) * chans, :]
        b_bar = ratio_same[g:g + 1] * b_in + ratio_cross[g:g + 1] * pltpu.roll(b_in, entries, 1)
        rows = slice(j * chans, (j + 1) * chans)
        cols = slice(j * lanes, (j + 1) * lanes)
        b_blocks[block, rows, cols] = b_bar.astype(jnp.bfloat16)
        c_blocks[block, rows, cols] = (
            c_ref[g * chans:(g + 1) * chans, :] * sign
        ).astype(jnp.bfloat16)

    loads["x"].wait()
    loads["w_in"].wait()
    mix_input = f32_dot(x_ref[...], w_in[...]).astype(jnp.bfloat16)
    loads["state"].wait()
    block_chans = per_block * chans
    activated = []
    for block in range(blocks):
        chan = slice(block * block_chans, (block + 1) * block_chans)
        inputs = mix_input[:, chan]
        forcing = f32_dot(inputs, b_blocks[block])
        following = []
        for j in range(per_block):
            g = block * per_block + j
            old = state[pl.ds(g, seqs, stride=groups), :]
            new = (
                bar_same[g:g + 1] * old
                + bar_cross[g:g + 1] * pltpu.roll(old, entries, 1)
                + forcing[:, j * lanes:(j + 1) * lanes]
            )
            new_state[pl.ds(g, seqs, stride=groups), :] = new
            following.append(new.astype(jnp.bfloat16))
        mixed = nt_dot(jnp.concatenate(following, 1), c_blocks[block])
        mixed = mixed + skip[chan].reshape(1, -1) * inputs.astype(jnp.float32)
        inner = math.sqrt(2.0 / math.pi) * (mixed + 0.044715 * mixed * mixed * mixed)
        activated.append((0.5 * mixed * (1.0 + jnp.tanh(inner))).astype(jnp.bfloat16))
    state_store = pltpu.make_async_copy(new_state, new_state_hbm, local_sem.at[9])
    state_store.start()
    activated = jnp.concatenate(activated, 1)

    loads["w_out"].wait()
    pl.semaphore_wait(barrier, 2 + n_ep)
    mix_copies = {}
    for k in (2, 3, 1):
        mix_send[k - 1] = f32_dot(activated, w_out[:, columns(peer[k])]).astype(jnp.bfloat16)
        mix_copies[k] = tp_copy(
            mix_send.at[k - 1], mix_recv.at[k - 1], mix_ss.at[k - 1], mix_rs.at[k - 1], k
        )
        mix_copies[k].start()
    own = f32_dot(activated, w_out[:, columns(tp)]).astype(jnp.bfloat16).astype(jnp.float32)
    per_group = w_expert.shape[0] // w_group.shape[0]
    chosen = routes[0:1, :] // per_group
    group_rows = -(-n_ep // 8) * 8
    in_group = jnp.where(
        chosen == lax.broadcasted_iota(jnp.int32, (group_rows, seqs), 0), 1.0, 0.0
    )
    earlier = jnp.where(
        lax.broadcasted_iota(jnp.int32, (seqs, seqs), 0)
        < lax.broadcasted_iota(jnp.int32, (seqs, seqs), 1),
        1.0,
        0.0,
    ).astype(jnp.bfloat16)
    prior = f32_dot(in_group.astype(jnp.bfloat16), earlier)
    rank = jnp.sum(prior * in_group, 0, keepdims=True)
    target = chosen.astype(jnp.float32) * cap + rank
    slot_row = lax.broadcasted_iota(jnp.int32, (slots, seqs), 0).astype(jnp.float32)
    slot_rows = jnp.where(target == slot_row, 1.0, 0.0)
    padded = slot_rows
    if seqs < slots:
        padded = jnp.concatenate(
            [slot_rows, jnp.zeros((slots, slots - seqs), jnp.float32)], 1
        )
    slot_map = padded.T.astype(jnp.bfloat16)
    slot_rows = slot_rows.astype(jnp.bfloat16)

    value = residual_scale * x_ref[:, columns(tp)].astype(jnp.float32) + own
    for k in (1, 2, 3):
        mix_copies[k].wait_recv()
        value = value + mix_recv[k - 1].astype(jnp.float32)

    def share_stats(value, buffer, send_sem, recv_sem, send_rows):
        mean = jnp.mean(value, -1, keepdims=True)
        centred = value - mean
        send_rows(centred.astype(jnp.bfloat16))
        square = jnp.sum(centred * centred, -1, keepdims=True)
        buffer[tp] = to_lanes([mean, square], seqs)
        copies = []
        for k in (2, 3, 1):
            copies.append(
                tp_copy(buffer.at[tp], buffer.at[tp], send_sem.at[k - 1], recv_sem.at[k - 1], k)
            )
            copies[-1].start()
        return centred, mean, copies

    def total_stats(buffer, copies):
        for copy in copies:
            copy.wait_recv()
        parts = [buffer[q] for q in range(n_tp)]
        means = [part[0:1] for part in parts]
        mean = sum(means) * (1.0 / n_tp)
        square = sum(part[1:2] for part in parts)
        square = square + quarter * sum((m - mean) * (m - mean) for m in means)
        return means, mean, lax.rsqrt(square * (1.0 / width) + norm_eps)

    if n_ep == 4:
        half = ep // 2
        targets = [3 * (1 - half), 2 - half, 1 - ep + 4 * half, ep]
    else:
        targets = [(ep + j) % n_ep for j in range(1, n_ep)] + [ep]
    nearest = targets[n_ep - 2::-1]

    go_copies = []

    def send_centred(rows):
        packed = f32_dot(slot_rows, rows).astype(jnp.bfloat16)
        for d in range(n_ep):
            go_rows[d] = packed[d * cap:(d + 1) * cap]
        for source in nearest:
            go_copies.append(
                pltpu.make_async_remote_copy(
                    src_ref=go_rows.at[source], dst_ref=rows_all.at[tp, ep],
                    send_sem=go_ss.at[source], recv_sem=go_rs.at[ep],
                    device_id={"ep": source}, device_id_type=MESH,
                )
            )
            go_copies[-1].start()

    centred, mean_own, mix_stat_copies = share_stats(
        value, stat_mix, stat_ss, stat_rs, send_centred
    )

    gather_sends = []

    def gather(source, way, k, q, piece):
        copy = tp_copy(
            piece, rows_all.at[q, source], gather_ss.at[way, source], gather_rs.at[way, source], k
        )
        copy.start()
        gather_sends.append(copy)

    def gather_wait(source, way, q):
        tp_copy(
            rows_all.at[q, source], rows_all.at[q, source],
            gather_ss.at[way, source], gather_rs.at[way, source], 1,
        ).wait_recv()

    rows_all[tp, ep] = go_rows[ep]
    gather(ep, 1, 2, tp, go_rows.at[ep])
    gather(ep, 0, 1, tp, go_rows.at[ep])
    means, mean, scale = total_stats(stat_mix, mix_stat_copies)
    line_row = lax.broadcasted_iota(jnp.int32, (8, 128), 0)
    lines = jnp.where(line_row == n_tp, scale, 0.0)
    for q in range(n_tp):
        lines = jnp.where(line_row == q, means[q] - mean, lines)
    split = []
    for _ in range(3):
        split.append(lines.astype(jnp.bfloat16))
        lines = lines - split[-1].astype(jnp.float32)
    split = f32_dot(jnp.concatenate([p.astype(jnp.float32) for p in split], 0).astype(jnp.bfloat16), slot_map)
    line_all[ep] = split[0:8] + split[8:16] + split[16:24]
    line_copies = []
    for j in (2, 1, 3) if n_ep == 4 else range(1, n_ep):
        line_copies.append(
            ep_copy(line_all.at[ep], line_all.at[ep], line_ss.at[j - 1], line_rs.at[j - 1], j)
        )
        line_copies[-1].start()
    back = to_columns([mean, scale], seqs)
    hidden_f32[...] = (centred + (mean_own - back[:, 0:1])) * back[:, 1:2] * gain_mix[:, columns(tp)]
    for source in nearest:
        ep_copy(
            go_rows.at[0], rows_all.at[tp, source], go_ss.at[source], go_rs.at[source], 1
        ).wait_recv()
        gather(source, 1, 2, tp, rows_all.at[tp, source])
        gather(source, 0, 1, tp, rows_all.at[tp, source])
    for source in [ep] + nearest:
        gather_wait(source, 1, peer[2])
        gather(source, 2, 1, peer[2], rows_all.at[peer[2], source])
    loads["gate"].wait()
    loads["up"].wait()
    loads["down"].wait()
    for source in [ep] + nearest:
        gather_wait(source, 0, peer[1])
        gather_wait(source, 2, peer[3])

    for j in range(1, n_ep):
        source = (ep + n_ep - j) % n_ep
        ep_copy(
            line_all.at[ep], line_all.at[source], line_ss.at[j - 1], line_rs.at[j - 1], j
        ).wait_recv()
    lines = [line_all[source] for source in range(n_ep)]
    if 8 * n_ep < 128:
        lines.append(jnp.zeros((128 - 8 * n_ep, 128), jnp.float32))
    line_columns[...] = jnp.concatenate(lines, 0).T
    mine = line_columns[pl.ds(pl.multiple_of(ep * cap, cap), cap), :]

    def line_column(at):
        return jnp.concatenate([mine[:, 8 * d + at:8 * d + at + 1] for d in range(n_ep)], 0)

    scale = line_column(n_tp)
    row_list = []
    for q in range(n_tp):
        part = rows_all[q].reshape(slots, quarter).astype(jnp.float32) + line_column(q)
        gain = gain_mix[:, q * quarter:(q + 1) * quarter]
        row_list.append((part * scale * gain).astype(jnp.bfloat16))
    row_list = jnp.concatenate(row_list, 1)
    group_logit = nt_dot(row_list, w_group[...])
    group_logit = group_logit - jnp.max(group_logit, -1, keepdims=True)
    group_exp = jnp.exp(group_logit)
    mine = lax.broadcasted_iota(jnp.int32, group_logit.shape, 1) == ep
    group_prob = jnp.sum(jnp.where(mine, group_exp, 0.0), -1, keepdims=True) / jnp.sum(
        group_exp, -1, keepdims=True
    )
    expert_logit = nt_dot(row_list, w_expert[...])
    expert_lane = lax.broadcasted_iota(jnp.int32, expert_logit.shape, 1)
    picked = [
        jnp.sum(jnp.where(expert_lane == ep * experts + e, expert_logit, 0.0), -1, keepdims=True)
        for e in range(experts)
    ]
    highest = functools.reduce(jnp.maximum, picked)
    picked = [jnp.exp(p - highest) for p in picked]
    share = group_prob / sum(picked)
    acts = []
    for e in range(experts):
        gate_val = f32_dot(row_list, w_gate[e])
        up_val = f32_dot(row_list, w_up[e])
        silu = gate_val * (0.5 + 0.5 * jnp.tanh(0.5 * gate_val))
        acts.append((silu * up_val * (picked[e] * share)).astype(jnp.bfloat16))
    acts = jnp.concatenate(acts, 1)

    core_copies = []
    for at, k in enumerate((3, 1)):
        core_send[at] = f32_dot(acts, w_down[:, columns(peer[k])]).astype(jnp.bfloat16)
        core_copies.append(
            tp_copy(core_send.at[at], core_recv.at[at], core_ss.at[at], core_rs.at[at], 1)
        )
        core_copies[-1].start()
    across = f32_dot(acts, w_down[:, columns(peer[2])])
    core_copies[0].wait_recv()
    cross_send[...] = (
        (across + core_recv[0].astype(jnp.float32)).astype(jnp.bfloat16).reshape(n_ep, cap, quarter)
    )
    cross_copies = {}
    for j, source in enumerate(targets):
        cross_copies[j] = tp_copy(
            cross_send.at[source], cross_recv.at[source],
            cross_ss.at[source], cross_rs.at[source], 2,
        )
        cross_copies[j].start()
    own = f32_dot(acts, w_down[:, columns(tp)])
    core_copies[1].wait_recv()
    back_send[...] = (own + core_recv[1].astype(jnp.float32)).reshape(n_ep, cap, quarter)
    back_copies = {}
    for j, source in enumerate(targets):
        cross_copies[j].wait_recv()
        total = (back_send[source] + cross_recv[source].astype(jnp.float32)).astype(jnp.bfloat16)
        if j == n_ep - 1:
            back_recv[ep] = total
        else:
            back_out[source] = total
            back_copies[j] = pltpu.make_async_remote_copy(
                src_ref=back_out.at[source], dst_ref=back_recv.at[ep],
                send_sem=back_ss.at[source], recv_sem=back_rs.at[ep],
                device_id={"ep": source}, device_id_type=MESH,
            )
            back_copies[j].start()
    for j in range(1, n_ep):
        source = (ep + n_ep - j) % n_ep
        ep_copy(
            back_out.at[0], back_recv.at[source], back_ss.at[source], back_rs.at[source], j
        ).wait_recv()

    moe = f32_dot(slot_map[:seqs], back_recv[...].reshape(slots, quarter))
    value = residual_scale * hidden_f32[...] + moe
    def last(way, k, q):
        copy = tp_copy(out_parts.at[q], out_parts.at[q], last_ss.at[way], last_rs.at[way], k)
        copy.start()
        return copy

    def last_wait(way, q):
        tp_copy(out_parts.at[q], out_parts.at[q], last_ss.at[way], last_rs.at[way], 1).wait_recv()

    last_copies = []

    def send_last(rows):
        out_parts[tp] = rows
        last_copies.extend([last(1, 2, tp), last(0, 1, tp)])

    _, _, out_stat_copies = share_stats(value, stat_out, stat2_ss, stat2_rs, send_last)
    last_wait(1, peer[2])
    last_copies.append(last(2, 1, peer[2]))
    means, mean, scale = total_stats(stat_out, out_stat_copies)
    back = to_columns([scale] + [m - mean for m in means], seqs)
    last_wait(0, peer[1])
    last_wait(2, peer[3])
    for q in range(n_tp):
        part = out_parts[q].astype(jnp.float32) + back[:, q + 1:q + 2]
        cols = slice(q * quarter, (q + 1) * quarter)
        out_ref[:, cols] = (part * back[:, 0:1] * gain_moe[:, cols]).astype(jnp.bfloat16)

    state_store.wait()
    sent = list(mix_copies.values()) + mix_stat_copies + go_copies + line_copies + gather_sends
    sent += core_copies + list(cross_copies.values()) + list(back_copies.values())
    for copy in sent + out_stat_copies + last_copies:
        copy.wait_send()


def store_kernel(pieces, out_in, state_in, out_ref, state_ref, out_held, state_held, load, store):
    rows = state_in.shape[0] // pieces
    moves = [(out_in, out_held, out_ref)]
    for at in range(pieces):
        part = pl.ds(at * rows, rows)
        moves.append((state_in.at[part], state_held.at[part], state_ref.at[part]))
    loads = [pltpu.make_async_copy(m[0], m[1], load.at[at]) for at, m in enumerate(moves)]
    stores = [pltpu.make_async_copy(m[1], m[2], store.at[at]) for at, m in enumerate(moves)]
    for copy in loads:
        copy.start()
    for at, copy in enumerate(loads):
        copy.wait()
        stores[at].start()
    for copy in stores:
        copy.wait()


def fused_device(
    x_in, state, routes, w_in, decay_rate, frequency, log_step, b_in, c_out, skip, w_out,
    gain_mix, w_group, w_expert, w_gate, w_up, w_down, gain_moe,
):
    seqs, width = x_in.shape
    groups, chans, lanes = b_in.shape
    mix_dev = w_in.shape[1]
    experts, _, ff = w_gate.shape
    n_ep = lax.axis_size("ep")
    n_tp = 4
    quarter = width // n_tp
    cap = max(2, 4 * seqs // w_expert.shape[1])
    per_block = 128 // chans
    blocks = groups // per_block
    bf16, f32 = jnp.bfloat16, jnp.float32
    vmem = pl.BlockSpec(memory_space=pltpu.VMEM)
    smem = pl.BlockSpec(memory_space=pltpu.SMEM)
    hbm = pl.BlockSpec(memory_space=pl.ANY)
    dma = pltpu.SemaphoreType.DMA
    layer_out, new_state = pl.pallas_call(
        fused_kernel,
        out_shape=(
            jax.ShapeDtypeStruct((seqs, width), bf16),
            jax.ShapeDtypeStruct((seqs * groups, lanes), f32),
        ),
        in_specs=[smem, hbm, hbm, vmem, hbm, vmem, vmem, hbm, hbm, vmem, hbm,
                  vmem, vmem, vmem, hbm, hbm, hbm, vmem],
        out_specs=(vmem, hbm),
        scratch_shapes=[
            pltpu.VMEM((seqs, width), bf16),
            pltpu.VMEM((seqs * groups, lanes), f32),
            pltpu.VMEM((seqs * groups, lanes), f32),
            pltpu.VMEM(w_in.shape, bf16),
            pltpu.VMEM(w_out.shape, bf16),
            pltpu.VMEM((groups * chans, lanes), f32),
            pltpu.VMEM((groups * chans, lanes), f32),
            pltpu.VMEM(w_gate.shape, bf16),
            pltpu.VMEM(w_up.shape, bf16),
            pltpu.VMEM((experts * ff, width), bf16),
            pltpu.VMEM((blocks, per_block * chans, per_block * lanes), bf16),
            pltpu.VMEM((blocks, per_block * chans, per_block * lanes), bf16),
            pltpu.VMEM((3, seqs, quarter), bf16),
            pltpu.VMEM((3, seqs, quarter), bf16),
            pltpu.VMEM((n_tp, 8, 128), f32),
            pltpu.VMEM((seqs, quarter), f32),
            pltpu.VMEM((n_ep, cap, quarter), bf16),
            pltpu.VMEM((n_tp, n_ep, cap, quarter), bf16),
            pltpu.VMEM((n_ep, 8, 128), f32),
            pltpu.VMEM((128, 128), f32),
            pltpu.VMEM((2, n_ep * cap, quarter), bf16),
            pltpu.VMEM((2, n_ep * cap, quarter), bf16),
            pltpu.VMEM((n_ep, cap, quarter), bf16),
            pltpu.VMEM((n_ep, cap, quarter), bf16),
            pltpu.VMEM((n_ep, cap, quarter), f32),
            pltpu.VMEM((n_ep, cap, quarter), bf16),
            pltpu.VMEM((n_ep, cap, quarter), bf16),
            pltpu.VMEM((n_tp, seqs, quarter), bf16),
            pltpu.VMEM((n_tp, 8, 128), f32),
            dma((10,)),
            dma((3,)), dma((3,)), dma((3,)), dma((3,)),
            dma((n_ep,)), dma((n_ep,)), dma((n_ep - 1,)), dma((n_ep - 1,)),
            dma((3, n_ep)), dma((3, n_ep)),
            dma((2,)), dma((2,)),
            dma((n_ep,)), dma((n_ep,)), dma((n_ep,)), dma((n_ep,)),
            dma((3,)), dma((3,)), dma((3,)), dma((3,)),
        ],
        compiler_params=pltpu.CompilerParams(collective_id=0, has_side_effects=True),
    )(
        log_step,
        x_in, state.reshape(seqs * groups, lanes), routes.T, w_in, decay_rate, frequency,
        b_in.reshape(groups * chans, lanes), c_out.reshape(groups * chans, lanes),
        skip, w_out, gain_mix.reshape(1, -1), w_group.T, w_expert.T,
        w_gate, w_up, w_down.reshape(experts * ff, width), gain_moe.reshape(1, -1),
    )
    pieces = 4
    layer_out, new_state = pl.pallas_call(
        functools.partial(store_kernel, pieces),
        out_shape=(
            jax.ShapeDtypeStruct((seqs, width), bf16),
            jax.ShapeDtypeStruct((seqs * groups, lanes), f32),
        ),
        in_specs=[hbm, hbm],
        out_specs=(hbm, hbm),
        scratch_shapes=[
            pltpu.VMEM((seqs, width), bf16),
            pltpu.VMEM((seqs * groups, lanes), f32),
            dma((pieces + 1,)), dma((pieces + 1,)),
        ],
    )(layer_out, new_state)
    return layer_out, new_state.reshape(seqs, groups, lanes)


def device_step(*args):
    x_in, routes, b_in, w_group, w_expert, w_gate = (
        args[0], args[2], args[7], args[12], args[13], args[14]
    )
    seqs, width = x_in.shape
    groups, chans, lanes = b_in.shape
    n_ep = lax.axis_size("ep")
    experts = w_gate.shape[0]
    per_group = w_expert.shape[1] // w_group.shape[1]
    cap = max(2, 4 * seqs // w_expert.shape[1])
    fits = (
        lax.axis_size("tp") == 4
        and per_group == experts == routes.shape[1]
        and n_ep > 1
        and n_ep * cap == 128
        and cap % 16 == 0
        and seqs <= 128
        and seqs % 16 == 0
        and width % 512 == 0
        and lanes == 128
        and 128 % chans == 0
        and chans % 16 == 0
        and groups % (128 // chans) == 0
    )
    return fused_device(*args) if fits else per_device(*args)


def solution(mesh):
    in_specs = (
        P(("grp", "ep"), None),
        P(("grp", "ep"), "tp", None),
        P(("grp", "ep"), None),
        P(None, "tp"),
        P("tp", None),
        P("tp", None),
        P("tp"),
        P("tp", None, None),
        P("tp", None, None),
        P("tp"),
        P("tp", None),
        P(),
        P(),
        P(),
        P("ep", None, "tp"),
        P("ep", None, "tp"),
        P("ep", "tp", None),
        P(),
    )
    out_specs = (P(("grp", "ep"), None), P(("grp", "ep"), "tp", None))
    return jax.shard_map(
        device_step, mesh=mesh, in_specs=in_specs, out_specs=out_specs, check_vma=False
    )
```

profile of v0, /device:TPU:0, one launch (start us, length us, event | category | flops | bytes accessed | tf_op | source)
XLA Modules:
  0.0 38.1 jit_solution(16771505057455688097)
XLA Ops:
  0.6 35.4 %shard_map.185 = (bf16[64,2048]{1,0:T(8,128)(2,1)}, f32[1536,128]{1,0:T(8,128)}) custom-call(f32[24]{0:T(128)} %log_step.1, bf16[64,2048]{1,0:T(8,128)(2,1)} %x_hbm.1, f32[1536,128]{1,0:T(8,128)} %bitcast.11, s32[2,64]{1,0:T(2,128)} %bitcast.18, bf16[2048,384]{1,0:T(8,128)(2,1)} %w_in_hbm.1, f32[24,64]{1,0:T(8,128)} %decay.1, f32[24,64]{1,0:T(8,128)} %freq.1, ...), custom_call_target="tpu_custom_call" | custom-call | tf_op jit(solution)/shard_map/pallas_call | solution.py:662
  36.1 2.0 %shard_map.186 = (bf16[64,2048]{1,0:T(8,128)(2,1)}, f32[1536,128]{1,0:T(8,128)}) custom-call(bf16[64,2048]{1,0:T(8,128)(2,1)} %get-tuple-element.6.out_in, f32[1536,128]{1,0:T(8,128)} %get-tuple-element.7.state_in), custom_call_target="tpu_custom_call" | custom-call | tf_op jit(solution)/shard_map/pallas_call | solution.py:718
where the time goes:
time: 38.4 us; the launch traced here: 38.1 us
  Pallas kernels  37.4 us (97%)
  between operations  0.65 us (2%)
    pallas_call x1, Pallas kernels, fused_device(): pl.pallas_call(fused_kernel, out_shape=(jax.ShapeDtypeStruct((seqs, width...  35.4 us
    pallas_call x1, Pallas kernels, fused_device(): pl.pallas_call(functools.partial(store_kernel, pieces), out_shape=(jax.Sh...  2.02 us

commit v1 on v0

--- a/solution.py
+++ b/solution.py
@@ -220,11 +220,12 @@
 
 
 def fused_kernel(
-    log_step,
-    x_hbm, state_hbm, routes, w_in_hbm, decay, freq, b_hbm, c_hbm, skip, w_out_hbm,
-    gain_mix, w_group, w_expert, w_gate_hbm, w_up_hbm, w_down_hbm, gain_moe,
-    out_ref, new_state_hbm,
-    x_ref, state, new_state, w_in, w_out, b_ref, c_ref, w_gate, w_up, w_down,
+    log_hbm, x_hbm, state_hbm, routes_hbm, w_in_hbm, decay_hbm, freq_hbm, b_hbm, c_hbm, skip_hbm,
+    w_out_hbm, gain_mix_hbm, w_group_hbm, w_expert_hbm, w_gate_hbm, w_up_hbm, w_down_hbm,
+    gain_moe_hbm,
+    out_ref, new_state,
+    log_step, decay, freq, skip, routes, gain_mix, w_group, w_expert, gain_moe,
+    x_ref, state, w_in, w_out, b_ref, c_ref, w_gate, w_up, w_down,
     b_blocks, c_blocks,
     mix_send, mix_recv, stat_mix, hidden_f32, go_rows, rows_all, line_all, line_columns,
     core_send, core_recv, cross_send, cross_recv, back_send, back_out, back_recv,
@@ -275,8 +276,12 @@
 
     loads = {}
     for at, (name, src, dst) in enumerate((
+        ("log", log_hbm, log_step), ("decay", decay_hbm, decay), ("freq", freq_hbm, freq),
         ("b", b_hbm, b_ref), ("c", c_hbm, c_ref), ("x", x_hbm, x_ref), ("w_in", w_in_hbm, w_in),
+        ("skip", skip_hbm, skip), ("routes", routes_hbm, routes), ("gain_mix", gain_mix_hbm, gain_mix),
         ("state", state_hbm, state), ("w_out", w_out_hbm, w_out),
+        ("w_group", w_group_hbm, w_group), ("w_expert", w_expert_hbm, w_expert),
+        ("gain_moe", gain_moe_hbm, gain_moe),
         ("gate", w_gate_hbm, w_gate), ("up", w_up_hbm, w_up), ("down", w_down_hbm, w_down),
     )):
         loads[name] = pltpu.make_async_copy(src, dst, local_sem.at[at])
@@ -290,10 +295,13 @@
             barrier, inc=1, device_id={"ep": (ep + j) % n_ep}, device_id_type=MESH
         )
 
-    group_row = lax.broadcasted_iota(jnp.int32, (groups, entries), 0)
-    step_log = jnp.zeros((groups, entries), jnp.float32)
-    for g in range(groups):
-        step_log = jnp.where(group_row == g, log_step[g], step_log)
+    loads["log"].wait()
+    loads["decay"].wait()
+    loads["freq"].wait()
+    own_group = lax.broadcasted_iota(jnp.int32, (groups, groups), 0) == lax.broadcasted_iota(
+        jnp.int32, (groups, groups), 1
+    )
+    step_log = jnp.sum(jnp.where(own_group, log_step[...], 0.0), 1, keepdims=True)
     step_size = jnp.exp(step_log)
     lam_real = -decay[...]
     lam_imag = freq[...]
@@ -332,6 +340,7 @@
     loads["w_in"].wait()
     mix_input = f32_dot(x_ref[...], w_in[...]).astype(jnp.bfloat16)
     loads["state"].wait()
+    loads["skip"].wait()
     block_chans = per_block * chans
     activated = []
     for block in range(blocks):
@@ -350,14 +359,13 @@
             new_state[pl.ds(g, seqs, stride=groups), :] = new
             following.append(new.astype(jnp.bfloat16))
         mixed = nt_dot(jnp.concatenate(following, 1), c_blocks[block])
-        mixed = mixed + skip[chan].reshape(1, -1) * inputs.astype(jnp.float32)
+        mixed = mixed + skip[block:block + 1, :] * inputs.astype(jnp.float32)
         inner = math.sqrt(2.0 / math.pi) * (mixed + 0.044715 * mixed * mixed * mixed)
         activated.append((0.5 * mixed * (1.0 + jnp.tanh(inner))).astype(jnp.bfloat16))
-    state_store = pltpu.make_async_copy(new_state, new_state_hbm, local_sem.at[9])
-    state_store.start()
     activated = jnp.concatenate(activated, 1)
 
-    loads["w_out"].wait()
+    for name in ("w_out", "routes", "gain_mix", "w_group", "w_expert", "gain_moe"):
+        loads[name].wait()
     pl.semaphore_wait(barrier, 2 + n_ep)
     mix_copies = {}
     for k in (2, 3, 1):
@@ -616,26 +624,19 @@
         cols = slice(q * quarter, (q + 1) * quarter)
         out_ref[:, cols] = (part * back[:, 0:1] * gain_moe[:, cols]).astype(jnp.bfloat16)
 
-    state_store.wait()
     sent = list(mix_copies.values()) + mix_stat_copies + go_copies + line_copies + gather_sends
     sent += core_copies + list(cross_copies.values()) + list(back_copies.values())
     for copy in sent + out_stat_copies + last_copies:
         copy.wait_send()
 
 
-def store_kernel(pieces, out_in, state_in, out_ref, state_ref, out_held, state_held, load, store):
-    rows = state_in.shape[0] // pieces
-    moves = [(out_in, out_held, out_ref)]
-    for at in range(pieces):
-        part = pl.ds(at * rows, rows)
-        moves.append((state_in.at[part], state_held.at[part], state_ref.at[part]))
-    loads = [pltpu.make_async_copy(m[0], m[1], load.at[at]) for at, m in enumerate(moves)]
-    stores = [pltpu.make_async_copy(m[1], m[2], store.at[at]) for at, m in enumerate(moves)]
-    for copy in loads:
+def store_kernel(out_in, state_in, out_ref, state_ref, store):
+    stores = [
+        pltpu.make_async_copy(state_in, state_ref, store.at[0]),
+        pltpu.make_async_copy(out_in, out_ref, store.at[1]),
+    ]
+    for copy in stores:
         copy.start()
-    for at, copy in enumerate(loads):
-        copy.wait()
-        stores[at].start()
     for copy in stores:
         copy.wait()
 
@@ -656,21 +657,27 @@
     blocks = groups // per_block
     bf16, f32 = jnp.bfloat16, jnp.float32
     vmem = pl.BlockSpec(memory_space=pltpu.VMEM)
-    smem = pl.BlockSpec(memory_space=pltpu.SMEM)
     hbm = pl.BlockSpec(memory_space=pl.ANY)
     dma = pltpu.SemaphoreType.DMA
     layer_out, new_state = pl.pallas_call(
         fused_kernel,
         out_shape=(
-            jax.ShapeDtypeStruct((seqs, width), bf16),
-            jax.ShapeDtypeStruct((seqs * groups, lanes), f32),
-        ),
-        in_specs=[smem, hbm, hbm, vmem, hbm, vmem, vmem, hbm, hbm, vmem, hbm,
-                  vmem, vmem, vmem, hbm, hbm, hbm, vmem],
-        out_specs=(vmem, hbm),
-        scratch_shapes=[
             pltpu.VMEM((seqs, width), bf16),
             pltpu.VMEM((seqs * groups, lanes), f32),
+        ),
+        in_specs=[hbm] * 18,
+        out_specs=(vmem, vmem),
+        scratch_shapes=[
+            pltpu.VMEM((1, groups), f32),
+            pltpu.VMEM(decay_rate.shape, f32),
+            pltpu.VMEM(decay_rate.shape, f32),
+            pltpu.VMEM((blocks, mix_dev // blocks), f32),
+            pltpu.VMEM((2, seqs), jnp.int32),
+            pltpu.VMEM((1, width), f32),
+            pltpu.VMEM((w_group.shape[1], width), bf16),
+            pltpu.VMEM((w_expert.shape[1], width), bf16),
+            pltpu.VMEM((1, width), f32),
+            pltpu.VMEM((seqs, width), bf16),
             pltpu.VMEM((seqs * groups, lanes), f32),
             pltpu.VMEM(w_in.shape, bf16),
             pltpu.VMEM(w_out.shape, bf16),
@@ -698,7 +705,7 @@
             pltpu.VMEM((n_ep, cap, quarter), bf16),
             pltpu.VMEM((n_tp, seqs, quarter), bf16),
             pltpu.VMEM((n_tp, 8, 128), f32),
-            dma((10,)),
+            dma((18,)),
             dma((3,)), dma((3,)), dma((3,)), dma((3,)),
             dma((n_ep,)), dma((n_ep,)), dma((n_ep - 1,)), dma((n_ep - 1,)),
             dma((3, n_ep)), dma((3, n_ep)),
@@ -708,27 +715,25 @@
         ],
         compiler_params=pltpu.CompilerParams(collective_id=0, has_side_effects=True),
     )(
-        log_step,
+        log_step.reshape(1, -1),
         x_in, state.reshape(seqs * groups, lanes), routes.T, w_in, decay_rate, frequency,
         b_in.reshape(groups * chans, lanes), c_out.reshape(groups * chans, lanes),
-        skip, w_out, gain_mix.reshape(1, -1), w_group.T, w_expert.T,
+        skip.reshape(blocks, -1), w_out, gain_mix.reshape(1, -1), w_group.T, w_expert.T,
         w_gate, w_up, w_down.reshape(experts * ff, width), gain_moe.reshape(1, -1),
     )
-    pieces = 4
     layer_out, new_state = pl.pallas_call(
-        functools.partial(store_kernel, pieces),
+        store_kernel,
         out_shape=(
             jax.ShapeDtypeStruct((seqs, width), bf16),
             jax.ShapeDtypeStruct((seqs * groups, lanes), f32),
         ),
-        in_specs=[hbm, hbm],
+        in_specs=[vmem, vmem],
         out_specs=(hbm, hbm),
-        scratch_shapes=[
-            pltpu.VMEM((seqs, width), bf16),
-            pltpu.VMEM((seqs * groups, lanes), f32),
-            dma((pieces + 1,)), dma((pieces + 1,)),
-        ],
-    )(layer_out, new_state)
+        scratch_shapes=[dma((2,))],
+    )(
+        pltpu.with_memory_space_constraint(layer_out, pltpu.VMEM),
+        pltpu.with_memory_space_constraint(new_state, pltpu.VMEM),
+    )
     return layer_out, new_state.reshape(seqs, groups, lanes)
 
 

time: 38.4 us -> 35.8 us (0.932)
  Pallas kernels: 37.4 us -> 34.9 us
    pallas_call x2, Pallas kernels: 37.4 us -> 34.9 us  [the longest x1 34 us: fused_device(): pl.pallas_call(fused_kernel, out_shape=(pltpu.VMEM((seqs, width), bf16),...]
where the time goes in v1:
time: 35.8 us; the launch traced here: 35.6 us
  Pallas kernels  34.9 us (97%)
  between operations  0.65 us (2%)
    pallas_call x1, Pallas kernels, fused_device(): pl.pallas_call(fused_kernel, out_shape=(pltpu.VMEM((seqs, width), bf16),...  34 us
    pallas_call x1, Pallas kernels, fused_device(): pl.pallas_call(store_kernel, out_shape=(jax.ShapeDtypeStruct((seqs, width...  0.98 us

profile of v1, /device:TPU:0, one launch (start us, length us, event | category | flops | bytes accessed | tf_op | source)
XLA Modules:
  0.0 35.6 jit_solution(6698040881074841950)
XLA Ops:
  0.6 34.0 %shard_map.185 = (bf16[64,2048]{1,0:T(8,128)(2,1)S(1)}, f32[1536,128]{1,0:T(8,128)S(1)}) custom-call(f32[1,24]{1,0:T(1,128)} %bitcast.22, bf16[64,2048]{1,0:T(8,128)(2,1)} %x_hbm.1, f32[1536,128]{1,0:T(8,128)} %bitcast.13, s32[2,64]{1,0:T(2,128)} %bitcast.21, bf16[2048,384]{1,0:T(8,128)(2,1)} %w_in_hbm.1, f32[24,64]{1,0:T(8,128)} %decay_hbm.1, ...), custom_call_target="tpu_custom_call" | custom-call | tf_op jit(solution)/shard_map/pallas_call | solution.py:662
  34.6 1.0 %shard_map.186 = (bf16[64,2048]{1,0:T(8,128)(2,1)}, f32[1536,128]{1,0:T(8,128)}) custom-call(bf16[64,2048]{1,0:T(8,128)(2,1)S(1)} %get-tuple-element.6.out_in, f32[1536,128]{1,0:T(8,128)S(1)} %get-tuple-element.7.state_in), custom_call_target="tpu_custom_call" | custom-call | tf_op jit(solution)/shard_map/pallas_call | solution.py:724
